TPU v7x, 32 devices: a whole 2x2x4 slice. The times are simulated.
32 devices in a mesh: grp: 2 (over y), fs: 4 (over z), tp: 4 (over x, core).
Axes of the slice: x: 2, y: 2, z: 4, core: 2. Of those that a mesh axis runs over, the one named last changes fastest.
Arguments:
- tokens: bfloat16 [4096, 2048], P(('grp', 'fs'), 'tp'), parts along dimension 0, may hold values from -36 to 36
- query_matrix: bfloat16 [2048, 1024], P('fs', 'tp'), may hold values from -0.125 to 0.125
- key_weight: bfloat16 [2048, 1024], P('fs', 'tp'), may hold values from -0.125 to 0.125
- value_weight: bfloat16 [2048, 2048], P('fs', 'tp'), may hold values from -0.125 to 0.125
- forget_lower_factor: bfloat16 [2048, 32], replicated, may hold values from -0.125 to 0.125
- decay_up: bfloat16 [32, 1024], replicated, may hold values from -1 to 1
- decay_bias: float32 [1024], replicated, may hold values from -1 to 8
- log_extra: float32 [4096, 1024], P(('grp', 'fs'), 'tp'), parts along dimension 0, may hold values from -0.7 to 0
- head_gain: float32 [256], replicated, may hold values from 0.1 to 1.9
- out_weight: bfloat16 [2048, 2048], P('tp', 'fs'), may hold values from -0.125 to 0.125
- mix_gain: float32 [2048], P('tp'), may hold values from 0.1 to 1.9
- up_weight: bfloat16 [2048, 8192], P('fs', 'tp'), may hold values from -0.125 to 0.125
- down_weight: bfloat16 [8192, 2048], P('tp', 'fs'), may hold values from -0.0625 to 0.0625
- out_gain: float32 [2048], P('tp'), may hold values from 0.1 to 1.9
Outputs:
- layer_out: bfloat16 [4096, 2048], P(('grp', 'fs'), 'tp'), parts along dimension 0
There are 2 independent parts, one for each index of `grp`. A program takes and returns all parts, laid end to end along the dimension named above; an argument that names none is the same for every part. Nothing has to cross between parts.
All inputs are finite; a program needn't handle non-finite values.
Results may differ from a plain program's by a relative error of at most 0.015.
Values may be sent and summed in bfloat16 or wider, within the bound.
A program may use at most 64 MiB of HBM per device.

v0:
```python
import jax
import jax.numpy as jnp
from jax import lax
from jax.sharding import PartitionSpec as P

D = 2048
DK = 128
DV = 256
SEGMENT_LENGTH = 64
ALPHA = 2.0**0.5
TAU = 16.0
EPS = 1e-05
HIGH = lax.Precision.HIGHEST


def block_scan(queries, key_rows, value_rows, log_decay):
    span = queries.shape[2]
    causal = (jnp.arange(span)[:, None] >= jnp.arange(span)[None, :])[:, :, None]

    def step(state, inputs):
        query_block, key_block, value_block, decay_block = inputs
        cumul = jnp.cumsum(decay_block, axis=1)
        last_cum = cumul[:, -1:, :]
        carried = jnp.einsum("hcd,hde->hce", query_block * jnp.exp(cumul), state, precision=HIGH)
        differ = cumul[:, :, None, :] - cumul[:, None, :, :]
        weights = jnp.exp(jnp.where(causal, differ, -jnp.inf))
        scores = jnp.sum(query_block[:, :, None, :] * key_block[:, None, :, :] * weights, axis=-1)
        within = jnp.einsum("hij,hje->hie", scores, value_block, precision=HIGH)
        fresh = jnp.einsum(
            "hcd,hce->hde", key_block * jnp.exp(last_cum - cumul), value_block, precision=HIGH
        )
        new_state = jnp.exp(last_cum[:, 0, :])[:, :, None] * state + fresh
        return (new_state, carried + within)

    start = jnp.zeros((queries.shape[1], queries.shape[3], value_rows.shape[3]), jnp.float32)
    _, outputs = lax.scan(step, start, (queries, key_rows, value_rows, log_decay))
    return outputs


def layer_norm(summed, gain_cols):
    row_total, row_squares = lax.psum(
        (jnp.sum(summed, axis=1), jnp.sum(summed * summed, axis=1)), "tp"
    )
    row_mean = row_total / D
    row_var = row_squares / D - row_mean * row_mean
    centered = summed - row_mean[:, None]
    return (centered * lax.rsqrt(row_var[:, None] + EPS) * gain_cols).astype(jnp.bfloat16)


def local(
    tokens,
    query_matrix,
    key_weight,
    value_weight,
    forget_lower_factor,
    decay_up,
    decay_bias,
    log_extra,
    head_gain,
    out_weight,
    mix_gain,
    up_weight,
    down_weight,
    out_gain,
):
    gathered = lax.all_gather(tokens, "tp", axis=1, tiled=True)
    row_count = gathered.shape[0]
    key_cols = query_matrix.shape[1]
    value_cols = value_weight.shape[1]
    local_heads = key_cols // DK
    block_pieces = (
        lax.all_gather(query_matrix, "fs", axis=0, tiled=True),
        lax.all_gather(key_weight, "fs", axis=0, tiled=True),
        lax.all_gather(value_weight, "fs", axis=0, tiled=True),
    )
    columns = gathered
    queries, key_rows, value_rows = tuple(
        (
            jnp.dot(columns, shard_piece, preferred_element_type=jnp.float32)
            for shard_piece in block_pieces
        )
    )
    queries = queries.astype(jnp.bfloat16)
    key_rows = key_rows.astype(jnp.bfloat16)
    value_rows = value_rows.astype(jnp.bfloat16)
    low = jnp.dot(gathered, forget_lower_factor, preferred_element_type=jnp.float32).astype(
        jnp.bfloat16
    )
    offset_cols = lax.axis_index("tp") * key_cols
    local_up = lax.dynamic_slice_in_dim(decay_up, offset_cols, key_cols, 1)
    local_bias = lax.dynamic_slice_in_dim(decay_bias, offset_cols, key_cols, 0)
    gate_pre = jnp.dot(low, local_up, preferred_element_type=jnp.float32) + local_bias
    log_decay = jax.nn.log_sigmoid(gate_pre) / TAU + log_extra
    count = row_count // SEGMENT_LENGTH

    def blocks(array, depth):
        return (
            array.astype(jnp.float32)
            .reshape(count, SEGMENT_LENGTH, local_heads, depth)
            .transpose(0, 2, 1, 3)
        )

    attended = block_scan(
        blocks(queries, DK) * DK ** (-0.5),
        blocks(key_rows, DK),
        blocks(value_rows, DV),
        blocks(log_decay, DK),
    )
    attended = attended.transpose(0, 2, 1, 3).reshape(row_count, local_heads, DV)
    scaled = (
        attended
        * lax.rsqrt(jnp.mean(attended * attended, axis=-1, keepdims=True) + EPS)
        * head_gain
    )
    mixed_heads = scaled.reshape(row_count, value_cols).astype(jnp.bfloat16)
    mix_terms = jnp.dot(
        mixed_heads,
        lax.all_gather(out_weight, "fs", axis=1, tiled=True),
        preferred_element_type=jnp.float32,
    )
    mix = lax.psum_scatter(
        mix_terms.astype(jnp.bfloat16), "tp", scatter_dimension=1, tiled=True
    ).astype(jnp.float32)
    normed_local = layer_norm(ALPHA * tokens.astype(jnp.float32) + mix, mix_gain)
    normed_rows = lax.all_gather(normed_local, "tp", axis=1, tiled=True)
    columns = normed_rows
    hidden = jnp.dot(
        columns,
        lax.all_gather(up_weight, "fs", axis=0, tiled=True),
        preferred_element_type=jnp.float32,
    )
    activation = jnp.square(jax.nn.relu(hidden)).astype(jnp.bfloat16)
    down_terms = jnp.dot(
        activation,
        lax.all_gather(down_weight, "fs", axis=1, tiled=True),
        preferred_element_type=jnp.float32,
    )
    down = lax.psum_scatter(
        down_terms.astype(jnp.bfloat16), "tp", scatter_dimension=1, tiled=True
    ).astype(jnp.float32)
    return layer_norm(ALPHA * normed_local.astype(jnp.float32) + down, out_gain)


def solution(mesh):
    in_specs = (
        P(("grp", "fs"), "tp"),
        P("fs", "tp"),
        P("fs", "tp"),
        P("fs", "tp"),
        P(),
        P(),
        P(),
        P(("grp", "fs"), "tp"),
        P(),
        P("tp", "fs"),
        P("tp"),
        P("fs", "tp"),
        P("tp", "fs"),
        P("tp"),
    )
    out_specs = P(("grp", "fs"), "tp")
    return jax.shard_map(local, mesh=mesh, in_specs=in_specs, out_specs=out_specs, check_vma=False)
```

profile of v0, /device:TPU:0, one launch (start us, length us, event | category | flops | bytes accessed | tf_op | source)
XLA Modules:
  0.0 615.8 jit_solution(9214274555413043903)
XLA Ops:
  10.8 23.4 %all-gather.9.cloned.1.call-done = bf16[512,2048]{1,0:T(8,128)(2,1)} async-done(((bf16[512,512]{1,0:T(8,128)(2,1)}), bf16[512,2048]{1,0:T(8,128)(2,1)}) %all-gather.9.cloned.1.call-update) | async-done | bytes 2097168 | tf_op jit(solution)/shard_map/all_gather | solution.py:66
  34.2 2.8 fusion.31
  38.1 25.7 %all-gather.15.cloned.1.call-done = bf16[2048,256]{1,0:T(8,128)(2,1)} async-done(((bf16[512,256]{1,0:T(8,128)(2,1)}), bf16[2048,256]{1,0:T(8,128)(2,1)}) %all-gather.15.cloned.1.call-update) | async-done | bytes 1048592 | tf_op jit(solution)/shard_map/all_gather | solution.py:72
  63.8 2.6 fusion.26
  67.4 25.3 %all-gather.11.cloned.1.call-done = bf16[2048,256]{1,0:T(8,128)(2,1)} async-done(((bf16[512,256]{1,0:T(8,128)(2,1)}), bf16[2048,256]{1,0:T(8,128)(2,1)}) %all-gather.11.cloned.1.call-update) | async-done | bytes 1048592 | tf_op jit(solution)/shard_map/all_gather | solution.py:73
  92.8 2.6 fusion.24
  96.4 42.9 %all-gather.13.cloned.1.call-done = bf16[2048,512]{1,0:T(8,128)(2,1)} async-done(((bf16[512,512]{1,0:T(8,128)(2,1)}), bf16[2048,512]{1,0:T(8,128)(2,1)}) %all-gather.13.cloned.1.call-update) | async-done | bytes 2097168 | tf_op jit(solution)/shard_map/all_gather | solution.py:74
  139.3 3.5 fusion.22
  145.6 38.5 %while.13 = (s32[]{:T(128)}, f32[2,128,256]{2,1,0:T(8,128)S(1)}, f32[8,2,64,256]{3,2,1,0:T(8,128)S(1)}, f32[8,2,64,128]{3,2,1,0:T(8,128)}, f32[8,2,64,128]{3,2,1...) while((s32[]{:T(128)}, f32[2,128,256]{2,1,0:T(8,128)S(1)}, ...), condition=%wide.region_3.4_spmd.clone, body=%wide.region_0.3_spmd.clone.sunk | while | flops 132444160 | bytes 2539644 | solution.py:36
  147.4 1.9 multiply_reduce_fusion.5
  152.2 1.9 multiply_reduce_fusion.5
  157.0 1.9 multiply_reduce_fusion.5
  161.8 1.9 multiply_reduce_fusion.5
  186.1 4.2 convolution_convert_fusion.1
  190.4 30.1 %reduce-scatter.3.cloned.1.call-done = bf16[512,512]{1,0:T(8,128)(2,1)} async-done(((bf16[512,2048]{1,0:T(8,128)(2,1)}), bf16[512,512]{1,0:T(8,128)(2,1)}) %reduce-scatter.3.cloned.1.call-update) | async-done | bytes 524304 | tf_op jit(solution)/shard_map/reduce_scatter | solution.py:121
  221.8 5.8 all-reduce.1
  227.6 2.1 multiply_convert_fusion.2
  231.4 21.6 %all-gather.19.cloned.1.call-done = bf16[512,2048]{1,0:T(8,128)(2,1)} async-done(((bf16[512,512]{1,0:T(8,128)(2,1)}), bf16[512,2048]{1,0:T(8,128)(2,1)}) %all-gather.19.cloned.1.call-update) | async-done | bytes 2097168 | tf_op jit(solution)/shard_map/all_gather | solution.py:125
  253.1 151.2 %all-gather.21.cloned.1.call-done = bf16[2048,2048]{1,0:T(8,128)(2,1)} async-done(((bf16[512,2048]{1,0:T(8,128)(2,1)}), bf16[2048,2048]{1,0:T(8,128)(2,1)}) %all-gather.21.cloned.1.call-update) | async-done | bytes 8388624 | tf_op jit(solution)/shard_map/all_gather | solution.py:129
  404.3 149.4 %all-gather.23.cloned.1.call-done = bf16[2048,2048]{1,0:T(8,128)(2,1)} async-done(((bf16[2048,512]{1,0:T(8,128)(2,1)}), bf16[2048,2048]{1,0:T(8,128)(2,1)}) %all-gather.23.cloned.1.call-update) | async-done | bytes 8388624 | tf_op jit(solution)/shard_map/all_gather | solution.py:135
  553.7 16.5 %convolution_convert_fusion = bf16[512,2048]{1,0:T(8,128)(2,1)} fusion(bf16[2048,2048]{1,0:T(8,128)(2,1)} %all-gather.23.cloned.1.call-done, bf16[512,2048]{1,0:T(8,128)(2,1)} %all-gather.19.cloned.1.call-done, bf16[2048,2048]{1,0:T(8,128)(2,1)} %all-gather.21.cloned.1.call-done), kind=kOutput, calls=%fused_computation.29 | convolution fusion | flops 8594128896 | bytes 20971520 | tf_op jit(solution)/shard_map/dot_general | solution.py:133
  570.2 29.5 %reduce-scatter.5.cloned.1.call-done = bf16[512,512]{1,0:T(8,128)(2,1)} async-done(((bf16[512,2048]{1,0:T(8,128)(2,1)}), bf16[512,512]{1,0:T(8,128)(2,1)}) %reduce-scatter.5.cloned.1.call-update) | async-done | bytes 524304 | tf_op jit(solution)/shard_map/reduce_scatter | solution.py:138
  601.1 5.8 all-reduce
  606.9 2.1 multiply_convert_fusion.1
  (138 shorter events, 46.9 us)
Async XLA Ops:
  6.5 27.7 %copy-start = (bf16[2048,32]{0,1:T(8,128)(2,1)S(1)}, bf16[2048,32]{0,1:T(8,128)(2,1)}, u32[]{:S(2)}) copy-start(bf16[2048,32]{0,1:T(8,128)(2,1)} %param.20) | copy-start | bytes 393220
  6.5 3.4 copy-start.7
  6.5 27.7 %copy-start.8 = (f32[512,256]{1,0:T(8,128)S(1)}, f32[512,256]{1,0:T(8,128)}, u32[]{:S(2)}) copy-start(f32[512,256]{1,0:T(8,128)} %param.23) | copy-start | bytes 1572868
  6.5 27.7 %all-gather.9.cloned.1.call-start = ((), (), s32[]{:S(2)}) async-start(), calls=%async_computation.2 | async-start | bytes 2621440 | tf_op jit(solution)/shard_map/all_gather | solution.py:66
  7.3 56.5 %all-gather.15.cloned.1.call-start = ((), (), s32[]{:S(2)}) async-start(), calls=%async_computation.5 | async-start | bytes 1310720 | tf_op jit(solution)/shard_map/all_gather | solution.py:72
  8.0 84.8 %all-gather.11.cloned.1.call-start = ((), (), s32[]{:S(2)}) async-start(), calls=%async_computation.3 | async-start | bytes 1310720 | tf_op jit(solution)/shard_map/all_gather | solution.py:73
  8.7 130.5 %all-gather.13.cloned.1.call-start = ((), (), s32[]{:S(2)}) async-start(), calls=%async_computation.4 | async-start | bytes 2621440 | tf_op jit(solution)/shard_map/all_gather | solution.py:74
  9.3 176.8 %all-gather.17.cloned.1.call-start = ((), (), s32[]{:S(2)}) async-start(), calls=%async_computation.6 | async-start | bytes 2621440 | tf_op jit(solution)/shard_map/all_gather | solution.py:118
  9.9 210.5 %reduce-scatter.3.cloned.1.call-start = ((), (), s32[]{:S(2)}) async-start(), calls=%async_computation.7 | async-start | bytes 2621440 | tf_op jit(solution)/shard_map/reduce_scatter | solution.py:121
  143.4 1.0 copy-start.3
  143.4 1.2 copy-start.4
  190.3 30.1 %copy-start.2 = (bf16[512,512]{1,0:T(8,128)(2,1)S(1)}, bf16[512,512]{1,0:T(8,128)(2,1)}, u32[]{:S(2)}) copy-start(bf16[512,512]{1,0:T(8,128)(2,1)} %param.16) | copy-start | bytes 1572868
  190.3 37.3 %copy-start.5 = (f32[512]{0:T(512)S(1)}, f32[512]{0:T(512)}, u32[]{:S(2)}) copy-start(f32[512]{0:T(512)} %param.26) | copy-start | bytes 6148
  190.3 62.7 %all-gather.19.cloned.1.call-start = ((), (), s32[]{:S(2)}) async-start(), calls=%async_computation.8 | async-start | bytes 2621440 | tf_op jit(solution)/shard_map/all_gather | solution.py:125
  229.7 174.6 %all-gather.21.cloned.1.call-start = ((), (), s32[]{:S(2)}) async-start(), calls=%async_computation.9 | async-start | bytes 10485760 | tf_op jit(solution)/shard_map/all_gather | solution.py:129
  230.5 323.2 %all-gather.23.cloned.1.call-start = ((), (), s32[]{:S(2)}) async-start(), calls=%async_computation.10 | async-start | bytes 10485760 | tf_op jit(solution)/shard_map/all_gather | solution.py:135
  231.2 368.5 %reduce-scatter.5.cloned.1.call-start = ((), (), s32[]{:S(2)}) async-start(), calls=%async_computation.11 | async-start | bytes 2621440 | tf_op jit(solution)/shard_map/reduce_scatter | solution.py:138
  570.2 29.5 %copy-start.1 = (bf16[512,512]{1,0:T(8,128)(2,1)S(1)}, bf16[512,512]{1,0:T(8,128)(2,1)}, u32[]{:S(2)}) copy-start(bf16[512,512]{1,0:T(8,128)(2,1)} %multiply_convert_fusion.2) | copy-start | bytes 1572868
  570.2 36.7 %copy-start.6 = (f32[512]{0:T(512)S(1)}, f32[512]{0:T(512)}, u32[]{:S(2)}) copy-start(f32[512]{0:T(512)} %param.29) | copy-start | bytes 6148
Sparse Core Ops, SparseCore 0:
  8.9 25.2 all-gather.8
  35.8 27.9 all-gather.14
  65.4 27.3 all-gather.10
  94.2 45.0 all-gather.12
  140.7 44.4 all-gather.16
  190.4 29.9 reduce-scatter.2
  229.8 23.1 all-gather.18
  254.6 149.6 all-gather.20
  405.8 147.7 all-gather.22
  570.3 29.3 reduce-scatter.4
where the time goes:
time: 617 us; the launch traced here: 616 us
  waiting for transfers between devices  504 us (82%)
  matrix products  39.9 us (6%)
  other arithmetic  23.6 us (4%)
  local copies, waits for them, and re-layouts  22.3 us (4%)
  between operations  13.7 us (2%)
  blocking collectives  11.5 us (2%)
    all_gather x1, waiting for transfers between devices, local(): lax.all_gather(up_weight, 'fs', axis=0, tiled=True)  151 us
    all_gather x1, waiting for transfers between devices, local(): lax.all_gather(down_weight, 'fs', axis=1, tiled=True)  149 us
    all_gather x1, waiting for transfers between devices, local(): lax.all_gather(value_weight, 'fs', axis=0, tiled=True)  42.9 us
    reduce_scatter x1, waiting for transfers between devices, local(): lax.psum_scatter(mix_terms.astype(jnp.bfloat16), 'tp', scatter_dimension=...  30.1 us
    reduce_scatter x1, waiting for transfers between devices, local(): lax.psum_scatter(down_terms.astype(jnp.bfloat16), 'tp', scatter_dimension...  29.5 us
    all_gather x1, waiting for transfers between devices, local(): lax.all_gather(query_matrix, 'fs', axis=0, tiled=True)  25.7 us
    all_gather x1, waiting for transfers between devices, local(): lax.all_gather(key_weight, 'fs', axis=0, tiled=True)  25.3 us
    all_gather x1, waiting for transfers between devices, local(): gathered = lax.all_gather(tokens, 'tp', axis=1, tiled=True)  23.4 us
  transfers between devices with their start and end apart: 10, of which 9 were waited for; matrix products, arithmetic and copies ran while one was open for 9% of the time, Pallas kernels for 0%

commit v1 on v0

--- a/solution.py
+++ b/solution.py
@@ -11,6 +11,17 @@
 TAU = 16.0
 EPS = 1e-05
 HIGH = lax.Precision.HIGHEST
+
+
+def collect(x, axis, dim):
+    ways = lax.axis_size(axis)
+    pieces = [x]
+    for far in range(1, ways):
+        pieces.append(
+            lax.ppermute(pieces[far - 1], axis, [(d, (d - 1) % ways) for d in range(ways)])
+        )
+    line = jnp.concatenate(pieces, axis=dim)
+    return jnp.roll(line, lax.axis_index(axis) * x.shape[dim], axis=dim)
 
 
 def block_scan(queries, key_rows, value_rows, log_decay):
@@ -71,7 +82,7 @@
     block_pieces = (
         lax.all_gather(query_matrix, "fs", axis=0, tiled=True),
         lax.all_gather(key_weight, "fs", axis=0, tiled=True),
-        lax.all_gather(value_weight, "fs", axis=0, tiled=True),
+        collect(value_weight, "fs", 0),
     )
     columns = gathered
     queries, key_rows, value_rows = tuple(

time: 617 us -> 580 us (0.940)
  waiting for transfers between devices: 504 us -> 442 us
  starting transfers between devices: 0.53 us -> 13.9 us
  local copies, waits for them, and re-layouts: 22.3 us -> 32.4 us
    all_gather x1 -> x0, waiting for transfers between devices: 42.9 us -> none  [local(): lax.all_gather(value_weight, 'fs', axis=0, tiled=True)]
    ppermute x0 -> x3, waiting for transfers between devices: none -> 38.9 us  [collect(): lax.ppermute(pieces[far - 1], axis, [(d, (d - 1) % ways) for d in range(w...]
    all_gather x1, waiting for transfers between devices: 25.7 us -> 0.02 us  [local(): lax.all_gather(query_matrix, 'fs', axis=0, tiled=True)]
    all_gather x1, waiting for transfers between devices: 23.4 us -> 0.01 us  [local(): gathered = lax.all_gather(tokens, 'tp', axis=1, tiled=True)]
    ppermute x0 -> x3, starting transfers between devices: none -> 13.6 us  [collect(): lax.ppermute(pieces[far - 1], axis, [(d, (d - 1) % ways) for d in range(w...]
    all_gather x1, waiting for transfers between devices: 25.3 us -> 15.9 us  [local(): lax.all_gather(key_weight, 'fs', axis=0, tiled=True)]
    unnamed x22 -> x23, local copies, waits for them, and re-layouts: 1.24 us -> 8.83 us
    dynamic_slice x0 -> x8, local copies, waits for them, and re-layouts: none -> 7.38 us  [block_scan(): lax.scan(step, start, (queries, key_rows, value_rows, log_decay))]
  transfers between devices with their start and end apart: 10 -> 12, of which waited for: 9 -> 10; matrix products, arithmetic and copies ran while one was open for 9% -> 12% of each run, Pallas kernels for 0% -> 0%
where the time goes in v1:
time: 580 us; the launch traced here: 579 us
  waiting for transfers between devices  442 us (76%)
  matrix products  41.2 us (7%)
  local copies, waits for them, and re-layouts  32.4 us (6%)
  other arithmetic  23.6 us (4%)
  starting transfers between devices  13.9 us (2%)
  between operations  13.4 us (2%)
  blocking collectives  11.7 us (2%)
    all_gather x1, waiting for transfers between devices, local(): lax.all_gather(up_weight, 'fs', axis=0, tiled=True)  151 us
    all_gather x1, waiting for transfers between devices, local(): lax.all_gather(down_weight, 'fs', axis=1, tiled=True)  149 us
    ppermute x3, waiting for transfers between devices, collect(): lax.ppermute(pieces[far - 1], axis, [(d, (d - 1) % ways) for d in range(w...  38.9 us
    reduce_scatter x1, waiting for transfers between devices, local(): lax.psum_scatter(mix_terms.astype(jnp.bfloat16), 'tp', scatter_dimension=...  30.1 us
    reduce_scatter x1, waiting for transfers between devices, local(): lax.psum_scatter(down_terms.astype(jnp.bfloat16), 'tp', scatter_dimension...  29.5 us
    all_gather x1, waiting for transfers between devices, local(): normed_rows = lax.all_gather(normed_local, 'tp', axis=1, tiled=True)  21.8 us
    dot_general x1, matrix products, local(): jnp.dot(activation, lax.all_gather(down_weight, 'fs', axis=1, tiled=True)...  16.5 us
    all_gather x1, waiting for transfers between devices, local(): lax.all_gather(key_weight, 'fs', axis=0, tiled=True)  15.9 us
  transfers between devices with their start and end apart: 12, of which 10 were waited for; matrix products, arithmetic and copies ran while one was open for 12% of the time, Pallas kernels for 0%

profile of v1, /device:TPU:0, one launch (start us, length us, event | category | flops | bytes accessed | tf_op | source)
XLA Modules:
  0.0 578.6 jit_solution(9152169955665068302)
XLA Ops:
  8.8 5.1 collective-permute-start
  13.9 11.5 %collective-permute-done = bf16[512,512]{1,0:T(8,128)(2,1)S(1)} collective-permute-done((bf16[512,512]{1,0:T(8,128)(2,1)}, bf16[512,512]{1,0:T(8,128)(2,1)S(1)}, u32[]{:S(2)}, u32[]{:S(2)}) %collective-permute-start) | collective-permute-done | bytes 524320 | tf_op jit(solution)/shard_map/ppermute | solution.py:21
  25.4 4.2 collective-permute-start.1
  29.7 10.2 %collective-permute-done.1 = bf16[512,512]{1,0:T(8,128)(2,1)S(1)} collective-permute-done((bf16[512,512]{1,0:T(8,128)(2,1)S(1)}, bf16[512,512]{1,0:T(8,128)(2,1)S(1)}, u32[]{:S(2)}, u32[]{:S(2)}) %collective-permute-start.1) | collective-permute-done | bytes 524320 | tf_op jit(solution)/shard_map/ppermute | solution.py:21
  39.9 4.3 collective-permute-start.2
  49.2 17.2 %collective-permute-done.2 = bf16[512,512]{1,0:T(8,128)(2,1)} collective-permute-done((bf16[512,512]{1,0:T(8,128)(2,1)S(1)}, bf16[512,512]{1,0:T(8,128)(2,1)}, u32[]{:S(2)}, u32[]{:S(2)}) %collective-permute-start.2) | collective-permute-done | bytes 524320 | tf_op jit(solution)/shard_map/ppermute | solution.py:21
  72.7 4.5 fusion.24
  80.4 3.0 fusion.35
  83.7 2.6 fusion.30
  86.5 15.9 %all-gather.10.cloned.1.call-done = bf16[2048,256]{1,0:T(8,128)(2,1)} async-done(((bf16[512,256]{1,0:T(8,128)(2,1)}), bf16[2048,256]{1,0:T(8,128)(2,1)}) %all-gather.10.cloned.1.call-update) | async-done | bytes 1048592 | tf_op jit(solution)/shard_map/all_gather | solution.py:84
  102.4 2.6 fusion.28
  106.2 39.3 %while.13 = (s32[]{:T(128)}, f32[2,128,256]{2,1,0:T(8,128)S(1)}, f32[8,2,64,256]{3,2,1,0:T(8,128)S(1)}, f32[8,2,64,128]{3,2,1,0:T(8,128)S(1)}, f32[8,2,64,128]{3...) while((s32[]{:T(128)}, f32[2,128,256]{2,1,0:T(8,128)S(1)}, ...), condition=%wide.region_3.4_spmd.clone, body=%wide.region_0.3_spmd.clone.sunk | while | flops 132444160 | bytes 2799748 | solution.py:47
  121.9 1.9 multiply_reduce_fusion.5
  148.9 4.2 convolution_convert_fusion.1
  153.2 30.1 %reduce-scatter.3.cloned.1.call-done = bf16[512,512]{1,0:T(8,128)(2,1)} async-done(((bf16[512,2048]{1,0:T(8,128)(2,1)}), bf16[512,512]{1,0:T(8,128)(2,1)}) %reduce-scatter.3.cloned.1.call-update) | async-done | bytes 524304 | tf_op jit(solution)/shard_map/reduce_scatter | solution.py:132
  184.7 5.9 %all-reduce.1 = (f32[512]{0:T(512)S(1)}, f32[512]{0:T(512)S(1)}) all-reduce(f32[512]{0:T(512)S(1)} %get-tuple-element.112, f32[512]{0:T(512)S(1)} %get-tuple-element.111), channel_id=1, replica_groups=mesh['grp'=2,'fs'=4,'tp'=4] {'tp'}, use_global_device_ids=true, to_apply=%region_9.10 | all-reduce | flops 1024 | bytes 8192 | tf_op jit(solution)/shard_map/psum | solution.py:52
  190.7 2.1 multiply_convert_fusion.2
  194.4 21.8 %all-gather.16.cloned.1.call-done = bf16[512,2048]{1,0:T(8,128)(2,1)} async-done(((bf16[512,512]{1,0:T(8,128)(2,1)}), bf16[512,2048]{1,0:T(8,128)(2,1)}) %all-gather.16.cloned.1.call-update) | async-done | bytes 2097168 | tf_op jit(solution)/shard_map/all_gather | solution.py:136
  216.1 151.2 %all-gather.18.cloned.1.call-done = bf16[2048,2048]{1,0:T(8,128)(2,1)} async-done(((bf16[512,2048]{1,0:T(8,128)(2,1)}), bf16[2048,2048]{1,0:T(8,128)(2,1)}) %all-gather.18.cloned.1.call-update) | async-done | bytes 8388624 | tf_op jit(solution)/shard_map/all_gather | solution.py:140
  367.4 149.4 %all-gather.20.cloned.1.call-done = bf16[2048,2048]{1,0:T(8,128)(2,1)} async-done(((bf16[2048,512]{1,0:T(8,128)(2,1)}), bf16[2048,2048]{1,0:T(8,128)(2,1)}) %all-gather.20.cloned.1.call-update) | async-done | bytes 8388624 | tf_op jit(solution)/shard_map/all_gather | solution.py:146
  516.8 16.5 %convolution_convert_fusion = bf16[512,2048]{1,0:T(8,128)(2,1)} fusion(bf16[2048,2048]{1,0:T(8,128)(2,1)} %all-gather.20.cloned.1.call-done, bf16[512,2048]{1,0:T(8,128)(2,1)} %all-gather.16.cloned.1.call-done, bf16[2048,2048]{1,0:T(8,128)(2,1)} %all-gather.18.cloned.1.call-done), kind=kOutput, calls=%fused_computation.25 | convolution fusion | flops 8594128896 | bytes 20971520 | tf_op jit(solution)/shard_map/dot_general | solution.py:144
  533.3 29.5 %reduce-scatter.5.cloned.1.call-done = bf16[512,512]{1,0:T(8,128)(2,1)} async-done(((bf16[512,2048]{1,0:T(8,128)(2,1)}), bf16[512,512]{1,0:T(8,128)(2,1)}) %reduce-scatter.5.cloned.1.call-update) | async-done | bytes 524304 | tf_op jit(solution)/shard_map/reduce_scatter | solution.py:149
  564.2 5.8 all-reduce
  570.0 2.1 multiply_convert_fusion.1
  (151 shorter events, 63.0 us)
Async XLA Ops:
  6.5 73.8 %copy-start = (bf16[2048,32]{0,1:T(8,128)(2,1)S(1)}, bf16[2048,32]{0,1:T(8,128)(2,1)}, u32[]{:S(2)}) copy-start(bf16[2048,32]{0,1:T(8,128)(2,1)} %param.20) | copy-start | bytes 393220
  6.5 61.7 %copy-start.3 = (bf16[512,512]{1,0:T(8,128)(2,1)S(1)}, bf16[512,512]{1,0:T(8,128)(2,1)}, u32[]{:S(2)}) copy-start(bf16[512,512]{1,0:T(8,128)(2,1)} %param.19) | copy-start | bytes 1572868
  6.5 66.1 %all-gather.8.cloned.1.call-start = ((), (), s32[]{:S(2)}) async-start(), calls=%async_computation.2 | async-start | bytes 2621440 | tf_op jit(solution)/shard_map/all_gather | solution.py:77
  7.3 76.4 %all-gather.12.cloned.1.call-start = ((), (), s32[]{:S(2)}) async-start(), calls=%async_computation.4 | async-start | bytes 1310720 | tf_op jit(solution)/shard_map/all_gather | solution.py:83
  8.0 94.4 %all-gather.10.cloned.1.call-start = ((), (), s32[]{:S(2)}) async-start(), calls=%async_computation.3 | async-start | bytes 1310720 | tf_op jit(solution)/shard_map/all_gather | solution.py:84
  8.7 140.2 %all-gather.14.cloned.1.call-start = ((), (), s32[]{:S(2)}) async-start(), calls=%async_computation.5 | async-start | bytes 2621440 | tf_op jit(solution)/shard_map/all_gather | solution.py:129
  8.8 16.6 %collective-permute-start = (bf16[512,512]{1,0:T(8,128)(2,1)}, bf16[512,512]{1,0:T(8,128)(2,1)S(1)}, u32[]{:S(2)}, u32[]{:S(2)}) collective-permute-start(bf16[512,512]{1,0:T(8,128)(2,1)} %param.19), channel_id=1, source_target_pairs={{0,12},{4,0},{8,4},{12,8},{1,13},{5,1},{9,5},{13,9},{2,14},{6,2},{... | collective-permute-start | bytes 1572872 | tf_op jit(solution)/shard_map/ppermute | solution.py:21
  25.4 14.5 %collective-permute-start.1 = (bf16[512,512]{1,0:T(8,128)(2,1)S(1)}, bf16[512,512]{1,0:T(8,128)(2,1)S(1)}, u32[]{:S(2)}, u32[]{:S(2)}) collective-permute-start(bf16[512,512]{1,0:T(8,128)(2,1)S(1)} %collective-permute-done), channel_id=1, source_target_pairs={{0,12},{4,0},{8,4},{12,8},{1,13},{5,1},{9,5},{13,9},{2,14},{6,2},{... | collective-permute-start | bytes 1572872 | tf_op jit(solution)/shard_map/ppermute | solution.py:21
  29.6 153.7 %reduce-scatter.3.cloned.1.call-start = ((), (), s32[]{:S(2)}) async-start(), calls=%async_computation.6 | async-start | bytes 2621440 | tf_op jit(solution)/shard_map/reduce_scatter | solution.py:132
  39.9 26.4 %collective-permute-start.2 = (bf16[512,512]{1,0:T(8,128)(2,1)S(1)}, bf16[512,512]{1,0:T(8,128)(2,1)}, u32[]{:S(2)}, u32[]{:S(2)}) collective-permute-start(bf16[512,512]{1,0:T(8,128)(2,1)S(1)} %collective-permute-done.1), channel_id=1, source_target_pairs={{0,12},{4,0},{8,4},{12,8},{1,13},{5,1},{9,5},{13,9},{2,14},{6,2},{... | collective-permute-start | bytes 1572872 | tf_op jit(solution)/shard_map/ppermute | solution.py:21
  148.9 34.4 %copy-start.2 = (bf16[512,512]{1,0:T(8,128)(2,1)S(1)}, bf16[512,512]{1,0:T(8,128)(2,1)}, u32[]{:S(2)}) copy-start(bf16[512,512]{1,0:T(8,128)(2,1)} %param.16) | copy-start | bytes 1572868
  148.9 41.8 %copy-start.4 = (f32[512]{0:T(512)S(1)}, f32[512]{0:T(512)}, u32[]{:S(2)}) copy-start(f32[512]{0:T(512)} %param.26) | copy-start | bytes 6148
  153.2 63.0 %all-gather.16.cloned.1.call-start = ((), (), s32[]{:S(2)}) async-start(), calls=%async_computation.7 | async-start | bytes 2621440 | tf_op jit(solution)/shard_map/all_gather | solution.py:136
  192.8 174.6 %all-gather.18.cloned.1.call-start = ((), (), s32[]{:S(2)}) async-start(), calls=%async_computation.8 | async-start | bytes 10485760 | tf_op jit(solution)/shard_map/all_gather | solution.py:140
  193.5 323.2 %all-gather.20.cloned.1.call-start = ((), (), s32[]{:S(2)}) async-start(), calls=%async_computation.9 | async-start | bytes 10485760 | tf_op jit(solution)/shard_map/all_gather | solution.py:146
  194.3 368.5 %copy-start.1 = (bf16[512,512]{1,0:T(8,128)(2,1)S(1)}, bf16[512,512]{1,0:T(8,128)(2,1)}, u32[]{:S(2)}) copy-start(bf16[512,512]{1,0:T(8,128)(2,1)} %multiply_convert_fusion.2) | copy-start | bytes 1572868
  194.3 375.6 %copy-start.5 = (f32[512]{0:T(512)S(1)}, f32[512]{0:T(512)}, u32[]{:S(2)}) copy-start(f32[512]{0:T(512)} %param.29) | copy-start | bytes 6148
  194.3 368.5 %reduce-scatter.5.cloned.1.call-start = ((), (), s32[]{:S(2)}) async-start(), calls=%async_computation.10 | async-start | bytes 2621440 | tf_op jit(solution)/shard_map/reduce_scatter | solution.py:149
Sparse Core Ops, SparseCore 0:
  8.9 25.2 all-gather.7
  35.8 34.8 all-gather.11
  72.2 30.1 all-gather.9
  103.8 45.0 all-gather.13
  153.3 29.9 reduce-scatter.2
  192.9 23.1 all-gather.15
  217.7 149.6 all-gather.17
  368.9 147.7 all-gather.19
  533.4 29.3 reduce-scatter.4
